TPU v7x, 1024 devices: a whole 4x8x16 slice. The times are simulated.
1024 devices in a mesh: ep: 32 (over z, core), tp: 32 (over y, x).
Axes of the slice: x: 4, y: 8, z: 16, core: 2. Of those that a mesh axis runs over, the one named last changes fastest.
Arguments:
- tokens: bfloat16 [512, 4096], P('ep', 'tp'), may hold values from -40 to 40
- norm_gain: bfloat16 [4096], P('tp'), may hold values from 0.099609375 to 1.8984375
- routes: int32 [512, 4], P('ep'), may hold values from 0 to 31, all different within a row; in each aligned block of 16 rows (0 to 15, 16 to 31, ...) at most 4 rows name the same one
- route_weights: float32 [512, 4], P('ep'), may hold values from 0.05 to 1
- w_gate: bfloat16 [32, 4096, 4096], P('ep', None, 'tp'), may hold values from -0.25 to 0.25
- w_up: bfloat16 [32, 4096, 4096], P('ep', None, 'tp'), may hold values from -0.25 to 0.25
- w_down: bfloat16 [32, 4096, 4096], P('ep', 'tp'), may hold values from -0.0234375 to 0.0234375
Outputs:
- mixed: bfloat16 [512, 4096], P('ep', 'tp')
Inputs may be any that keep to these rules, and one draw needn't show every extreme that they name: `routes`: within the 16 rows of one device, each token names 4 different experts, and no expert is named by more than 4 rows; some expert reaches 4.
All inputs are finite; a program needn't handle non-finite values.
Results may differ from a plain program's by a relative error of at most 0.018.
Values may be sent and summed in bfloat16 or wider, within the bound.
A program may use at most 64 MiB of HBM per device.

v0:
```python
import jax
import jax.numpy as jnp
from jax import lax
from jax.sharding import PartitionSpec as P

D = 4096


def from_everyone(x, axis):
    copies = jnp.broadcast_to(x, (lax.axis_size(axis), *x.shape))
    return lax.all_to_all(copies, axis, split_axis=0, concat_axis=0, tiled=True)


def of_everyone(x, axis):
    everything = from_everyone(x, axis)
    return jnp.sum(everything, axis=0)


def laid_out(tiles, dim):
    tiles = jnp.moveaxis(tiles, 0, dim)
    shape = tiles.shape
    return tiles.reshape(*shape[:dim], shape[dim] * shape[dim + 1], *shape[dim + 2 :])


def gather_directly(x, axis, dim):
    return laid_out(from_everyone(x, axis), dim)


def in_blocks(x, dim, size):
    before, after = (x.shape[:dim], x.shape[dim + 1 :])
    return jnp.moveaxis(x.reshape(*before, size, -1, *after), dim, 0)


def sum_at_owner(x, axis, dim):
    tiles = in_blocks(x, dim, lax.axis_size(axis))
    arrived = lax.all_to_all(tiles, axis, split_axis=0, concat_axis=0, tiled=True)
    return arrived.astype(jnp.float32).sum(axis=0)


def shards(tokens, norm_gain, routes, route_weights, w_gate, w_up, w_down):
    tok_rows = tokens.shape[0]
    topk = routes.shape[1]
    groups = lax.axis_size("ep")
    capacity = min(tok_rows, max(2, 2 * tok_rows * topk // groups))
    slot_rows = groups * capacity
    flat = routes.reshape(-1)
    order = jnp.arange(flat.shape[0], dtype=jnp.int32)
    earlier = (flat[:, None] == flat[None, :]) & (order[:, None] > order[None, :])
    slot = jnp.sum(earlier.astype(jnp.int32), axis=1)
    target = (flat * capacity + slot).reshape(tok_rows, topk)
    slot_ids = jnp.arange(slot_rows, dtype=jnp.int32)
    picker = jnp.any(target[None, :, :] == slot_ids[:, None, None], axis=2).astype(jnp.bfloat16)
    combine = jnp.sum(
        jnp.where(target[:, :, None] == slot_ids[None, None, :], route_weights[:, :, None], 0.0),
        axis=1,
    )
    values = tokens.astype(jnp.float32)
    total_sq = of_everyone(jnp.sum(values * values, axis=1), "tp")
    scale = lax.rsqrt(total_sq / D + 1e-05)
    normed = (values * scale[:, None] * norm_gain.astype(jnp.float32)[None, :]).astype(jnp.bfloat16)
    outbound = jnp.dot(picker, normed, preferred_element_type=jnp.float32).astype(jnp.bfloat16)
    arrived = lax.all_to_all(
        outbound.reshape(groups, capacity, -1), "ep", split_axis=0, concat_axis=0, tiled=True
    ).reshape(slot_rows, -1)
    piece = gather_directly(arrived, "tp", 1)
    gate_rows = w_gate[0]
    up_rows = w_up[0]
    gate_pre = jnp.dot(piece, gate_rows, preferred_element_type=jnp.float32)
    up_pre = jnp.dot(piece, up_rows, preferred_element_type=jnp.float32)
    gated = jnp.minimum(gate_pre, 7.0)
    upper = jnp.clip(up_pre, -7.0, 7.0)
    hidden = ((upper + 1.0) * gated * jax.nn.sigmoid(1.702 * gated)).astype(jnp.bfloat16)
    partial_out = jnp.dot(hidden, w_down[0], preferred_element_type=jnp.float32).astype(
        jnp.bfloat16
    )
    summed = sum_at_owner(partial_out, "tp", 1).astype(jnp.bfloat16)
    returned = lax.all_to_all(
        summed.reshape(groups, capacity, -1), "ep", split_axis=0, concat_axis=0, tiled=True
    ).reshape(slot_rows, -1)
    mixed = jnp.dot(combine, returned.astype(jnp.float32), precision=lax.Precision.HIGHEST)
    return mixed.astype(jnp.bfloat16)


def solution(mesh):
    placed = (
        P("ep", "tp"),
        P("tp"),
        P("ep", None),
        P("ep", None),
        P("ep", None, "tp"),
        P("ep", None, "tp"),
        P("ep", "tp", None),
    )
    return jax.shard_map(
        shards, mesh=mesh, in_specs=placed, out_specs=P("ep", "tp"), check_vma=False
    )
```

profile of v0, /device:TPU:1, one launch (start us, length us, event | category | flops | bytes accessed | tf_op | source)
XLA Modules:
  0.0 139.3 jit_solution(18245676942602241685)
XLA Ops:
  0.0 0.9 fusion.20
  0.9 0.6 broadcast_in_dim.27
  1.5 10.5 %all-to-all-start = ((f32[32,1,16]{2,1,0:T(1,128)}), f32[32,1,16]{2,1,0:T(1,128)S(1)}, u32[]{:S(2)}, u32[]{:S(2)}) async-start(f32[32,1,16]{2,1,0:T(1,128)} %broadcast_in_dim.27), calls=%async_computation | async-start | bytes 32768 | tf_op jit(solution)/shard_map/all_to_all | solution.py:11
  12.0 0.8 copy.33
  12.8 0.1 eq.20
  12.8 0.2 convert_reduce_fusion
  13.0 0.1 reduce_sum.51
  13.1 0.1 copy.34
  13.2 0.7 multiply_add_fusion
  14.0 0.7 convert_element_type.30
  14.6 6.0 %all-to-all-done = f32[32,1,16]{2,1,0:T(1,128)S(1)} async-done(((f32[32,1,16]{2,1,0:T(1,128)}), f32[32,1,16]{2,1,0:T(1,128)S(1)}, u32[]{:S(2)}, u32[]{:S(2)}) %all-to-all-start) | async-done | bytes 2080 | tf_op jit(solution)/shard_map/all_to_all | solution.py:11
  20.7 0.9 convolution_convert_fusion.1
  21.6 32.7 %all_to_all.26 = bf16[32,4,128]{2,1,0:T(4,128)(2,1)S(1)} all-to-all(bf16[32,4,128]{2,1,0:T(4,128)(2,1)S(1)} %bitcast.35), channel_id=1, replica_groups=mesh['ep'=32,'tp'=32] {'ep'}, dimensions={0} | all-to-all | bytes 65536 | tf_op jit(solution)/shard_map/all_to_all | solution.py:62
  54.3 0.1 copy.36
  54.4 0.2 broadcast_in_dim.28
  54.7 29.2 %all_to_all.27 = bf16[32,128,128]{1,2,0:T(8,128)(2,1)S(1)} all-to-all(bf16[32,128,128]{1,2,0:T(8,128)(2,1)S(1)} %broadcast_in_dim.28), channel_id=1, replica_groups=mesh['ep'=32,'tp'=32] {'tp'}, dimensions={0} | all-to-all | bytes 2097152 | tf_op jit(solution)/shard_map/all_to_all | solution.py:11
  83.8 0.5 convolution_minimum_fusion
  84.4 2.1 %fusion = bf16[16,32,8,128]{3,2,1,0:T(8,128)(2,1)S(1)} fusion(f32[128,128]{1,0:T(8,128)S(1)} %convolution_minimum_fusion, bf16[128,4096]{0,1:T(8,128)(2,1)S(1)} %bitcast.31, bf16[1,128,4096]{2,1,0:T(8,128)(2,1)S(1)} %copy-done, bf16[1,4096,128]{2,1,0:T(8,128)(2,1)} %param.12), kind=kOutput, calls=%fused_computation.1 | convolution fusion | flops 269107200 | bytes 4259840 | tf_op jit(solution)/shard_map/dot_general | solution.py:73
  86.4 0.3 copy.41
  86.7 31.6 %all_to_all.28 = bf16[32,128,128]{2,1,0:T(8,128)(2,1)S(1)} all-to-all(bf16[32,128,128]{2,1,0:T(8,128)(2,1)S(1)} %bitcast.32), channel_id=1, replica_groups=mesh['ep'=32,'tp'=32] {'tp'}, dimensions={0} | all-to-all | bytes 2097152 | tf_op jit(solution)/shard_map/all_to_all | solution.py:36
  118.3 0.8 reduce_sum.55
  119.0 7.2 %all-to-all-start.4 = ((bf16[32,4,128]{2,1,0:T(4,128)(2,1)}), bf16[32,4,128]{2,1,0:T(4,128)(2,1)S(1)}, u32[]{:S(2)}, u32[]{:S(2)}) async-start(bf16[32,4,128]{2,1,0:T(4,128)(2,1)} %bitcast.9), calls=%async_computation.4 | async-start | bytes 65536 | tf_op jit(solution)/shard_map/all_to_all | solution.py:77
  126.3 12.2 %all-to-all-done.4 = bf16[32,4,128]{2,1,0:T(4,128)(2,1)S(1)} async-done(((bf16[32,4,128]{2,1,0:T(4,128)(2,1)}), bf16[32,4,128]{2,1,0:T(4,128)(2,1)S(1)}, u32[]{:S(2)}, u32[]{:S(2)}) %all-to-all-start.4) | async-done | bytes 32800 | tf_op jit(solution)/shard_map/all_to_all | solution.py:77
  138.5 0.7 convolution_convert_fusion.2
  (10 shorter events, 0.2 us)
Async XLA Ops:
  0.0 84.3 %copy-start = (bf16[1,128,4096]{2,1,0:T(8,128)(2,1)S(1)}, bf16[1,128,4096]{2,1,0:T(8,128)(2,1)}, u32[]{:S(2)}) copy-start(bf16[1,128,4096]{2,1,0:T(8,128)(2,1)} %param.13) | copy-start | bytes 3145732
  1.5 19.1 %all-to-all-start = ((f32[32,1,16]{2,1,0:T(1,128)}), f32[32,1,16]{2,1,0:T(1,128)S(1)}, u32[]{:S(2)}, u32[]{:S(2)}) async-start(f32[32,1,16]{2,1,0:T(1,128)} %broadcast_in_dim.27), calls=%async_computation | async-start | bytes 32768 | tf_op jit(solution)/shard_map/all_to_all | solution.py:11
  54.7 29.2 %copy-start.1 = (bf16[1,4096,128]{2,1,0:T(8,128)(2,1)S(1)}, bf16[1,4096,128]{2,1,0:T(8,128)(2,1)}, u32[]{:S(2)}) copy-start(bf16[1,4096,128]{2,1,0:T(8,128)(2,1)} %param.11) | copy-start | bytes 3145732
  118.3 8.0 %copy-start.2 = (f32[16,4]{0,1:T(4,128)S(1)}, f32[16,4]{0,1:T(4,128)}, u32[]{:S(2)}) copy-start(f32[16,4]{0,1:T(4,128)} %param.10) | copy-start | bytes 772
  119.0 19.5 %all-to-all-start.4 = ((bf16[32,4,128]{2,1,0:T(4,128)(2,1)}), bf16[32,4,128]{2,1,0:T(4,128)(2,1)S(1)}, u32[]{:S(2)}, u32[]{:S(2)}) async-start(bf16[32,4,128]{2,1,0:T(4,128)(2,1)} %bitcast.9), calls=%async_computation.4 | async-start | bytes 65536 | tf_op jit(solution)/shard_map/all_to_all | solution.py:77
where the time goes:
time: 140 us; the launch traced here: 139 us
  blocking collectives  93.4 us (67%)
  waiting for transfers between devices  18.1 us (13%)
  starting transfers between devices  17.7 us (13%)
  matrix products  4.23 us (3%)
  other arithmetic  3.39 us (2%)
  local copies, waits for them, and re-layouts  2.27 us (2%)
    all_to_all x1, blocking collectives, shards(): lax.all_to_all(outbound.reshape(groups, capacity, -1), 'ep', split_axis=0...  32.7 us
    all_to_all x1, blocking collectives, sum_at_owner(): lax.all_to_all(tiles, axis, split_axis=0, concat_axis=0, tiled=True)  31.6 us
    all_to_all x1, blocking collectives, from_everyone(): return lax.all_to_all(copies, axis, split_axis=0, concat_axis=0, tiled=True)  29.2 us
    all_to_all x1, waiting for transfers between devices, shards(): lax.all_to_all(summed.reshape(groups, capacity, -1), 'ep', split_axis=0,...  12.2 us
    all_to_all x1, starting transfers between devices, from_everyone(): return lax.all_to_all(copies, axis, split_axis=0, concat_axis=0, tiled=True)  10.5 us
    all_to_all x1, starting transfers between devices, shards(): lax.all_to_all(summed.reshape(groups, capacity, -1), 'ep', split_axis=0,...  7.2 us
    all_to_all x1, waiting for transfers between devices, from_everyone(): return lax.all_to_all(copies, axis, split_axis=0, concat_axis=0, tiled=True)  5.98 us
  transfers between devices with their start and end apart: 2, of which 2 were waited for; matrix products, arithmetic and copies ran while one was open for 2% of the time, Pallas kernels for 0%

commit v1 on v0

v1 whole, which is shorter than its diff:
```python
import functools

import jax
import jax.numpy as jnp
from jax import lax
from jax.experimental import pallas as pl
from jax.experimental.pallas import tpu as pltpu
from jax.sharding import PartitionSpec as P

MESH = pl.DeviceIdType.MESH
BF16 = jnp.bfloat16
F32 = jnp.float32
W = 128
CAP = 4
EPS = 1e-05


def by_distance(n):
    return sorted(range(n), key=lambda j: (min(j, n - j), j))


class Plan:
    def __init__(self, nz, ny, nx):
        self.nz, self.ny, self.nx = nz, ny, nx
        self.experts = 2 * nz
        self.tp = ny * nx
        self.d = self.tp * W
        ring = by_distance(nz)
        self.chunks = [ring[: nz // 2], ring[nz // 2 :]]
        self.pos = {j: at for at, j in enumerate(ring)}
        self.rows = (nz // 2) * 2 * CAP
        self.near = by_distance(ny)
        self.far = self.near[::-1]


def kernel(
    plan,
    tok,
    gain,
    routes,
    rw,
    wg,
    wu,
    wd,
    out,
    wgu_v,
    wd_v,
    ob,
    lb,
    G,
    GA,
    PB,
    XR,
    XM,
    SM,
    Q,
    YL,
    RB,
    RI,
    s_w,
    s_disp,
    r_disp,
    s_gy,
    r_gy,
    s_gx,
    r_gx,
    s_gr,
    r_gr,
    s_xr,
    r_xr,
    s_xm,
    r_xm,
    s_yl,
    r_yl,
    s_ret,
    r_ret,
):
    nz, ny, nx, rows = plan.nz, plan.ny, plan.nx, plan.rows
    ep = lax.axis_index("ep")
    tp = lax.axis_index("tp")
    z, c = ep // 2, ep % 2
    y, x = tp // nx, tp % nx
    right, left, across = (x + 1) % nx, (x + nx - 1) % nx, (x + 2) % nx

    def at_z(j):
        return (z + j) % nz

    def at_y(dy):
        return (y + dy) % ny

    def id_z(j, core):
        return (at_z(j) * 2 + core, tp)

    def id_y(dy):
        return (ep, at_y(dy) * nx + x)

    def id_x(xx):
        return (ep, y * nx + xx)

    peers = [id_z(j, core) for j in range(1, nz) for core in (0, 1)]
    peers += [id_z(0, 1 - c)]
    peers += [id_y(dy) for dy in range(1, ny)]
    peers += [id_x(right), id_x(left)]
    barrier = pltpu.get_barrier_semaphore()
    for peer in peers:
        pl.semaphore_signal(barrier, inc=1, device_id=peer, device_id_type=MESH)

    def weight_copies():
        copies = []
        for yy in range(ny):
            for xx in range(nx):
                block = yy * nx + xx
                for half, src in enumerate((wg, wu)):
                    copies.append(
                        pltpu.make_async_copy(
                            src.at[block],
                            wgu_v.at[xx, pl.ds(yy * W, W), pl.ds(half * W, W)],
                            s_w.at[half, block],
                        )
                    )
        copies.append(pltpu.make_async_copy(wd, wd_v, s_w.at[2, 0]))
        return copies

    weights = weight_copies()
    for copy in weights:
        copy.start()

    tokens = tok.shape[0]
    lanes = plan.experts * CAP
    slot_id = lax.broadcasted_iota(jnp.int32, (tokens, lanes), 1)
    expert_of = slot_id // CAP
    named = jnp.zeros((tokens, lanes), F32)
    weight = jnp.zeros((tokens, lanes), F32)
    for k in range(routes.shape[1]):
        same = routes[:, k : k + 1] == expert_of
        named = jnp.where(same, 1.0, named)
        weight = jnp.where(same, rw[:, k : k + 1], weight)
    lower = (
        lax.broadcasted_iota(jnp.int32, (tokens, tokens), 0)
        > lax.broadcasted_iota(jnp.int32, (tokens, tokens), 1)
    ).astype(F32)
    earlier = jnp.dot(lower, named, preferred_element_type=F32)
    pick = jnp.where(earlier == (slot_id % CAP).astype(F32), named, 0.0)
    combine = weight * pick
    outbound = lax.dot_general(
        pick.astype(BF16),
        tok[...],
        (((0,), (0,)), ((), ())),
        preferred_element_type=F32,
    )
    ob[...] = outbound.reshape(plan.experts, CAP, W).astype(BF16)
    GA[x, y] = jnp.broadcast_to(gain[...], (8, W))
    lb[c] = ob[ep]

    pending = []

    def remote(src, dst, send, recv, device):
        copy = pltpu.make_async_remote_copy(
            src_ref=src,
            dst_ref=dst,
            send_sem=send,
            recv_sem=recv,
            device_id=device,
            device_id_type=MESH,
        )
        copy.start()
        pending.append(copy)
        return copy

    def arrive(ref, sem):
        pltpu.make_async_copy(ref, ref, sem).wait()

    pl.semaphore_wait(barrier, len(peers))

    for j in by_distance(nz)[::-1]:
        landing = plan.pos[(-j) % nz] * 2 + c
        for core in (0, 1) if j else (1 - c,):
            target = at_z(j) * 2 + core
            index = 2 * plan.pos[(-j) % nz] + (core if j else 0)
            remote(
                ob.at[target],
                lb.at[landing],
                s_disp.at[index],
                r_disp.at[landing],
                (target, tp),
            )

    def gather_y(buf, n):
        for dy in plan.far[:-1]:
            remote(buf.at[x, y], buf.at[x, y], s_gy.at[n, dy], r_gy.at[n, (-dy) % ny], id_y(dy))

    def gather_x(buf, n):
        for at, dy in enumerate(plan.near):
            here = buf.at[x, at_y(dy)]
            if dy:
                arrive(here, r_gy.at[n, dy])
            remote(here, here, s_gx.at[n, 0, dy], r_gx.at[n, 0, dy], id_x(right))
            remote(here, here, s_gx.at[n, 1, dy], r_gx.at[n, 1, dy], id_x(left))

    def gather_relay(buf, n):
        for at, dy in enumerate(plan.near):
            way = at % 2
            source, target = (left, right) if way == 0 else (right, left)
            here = buf.at[source, at_y(dy)]
            arrive(here, r_gx.at[n, way, dy])
            remote(here, here, s_gr.at[n, dy], r_gr.at[n, dy], id_x(target))

    def gather_rest(buf, n, which):
        for at, dy in enumerate(plan.near):
            if which == "sides":
                way = 1 - at % 2
                source = left if way == 0 else right
                arrive(buf.at[source, at_y(dy)], r_gx.at[n, way, dy])
            else:
                arrive(buf.at[across, at_y(dy)], r_gr.at[n, dy])

    def chunk_in(k):
        for at in range(len(plan.chunks[k])):
            j = plan.chunks[k][at]
            base = plan.pos[j] * 2
            if j:
                for core in (0, 1):
                    arrive(lb.at[base + core], r_disp.at[base + core])
            else:
                arrive(lb.at[base + 1 - c], r_disp.at[base + 1 - c])
        groups = rows // CAP
        G[k, x, y] = lb[k * groups : (k + 1) * groups].reshape(rows, W)

    def part(k, xx):
        pieces, square = [], jnp.zeros((rows, W), F32)
        for yy in range(ny):
            piece = G[k, xx, yy]
            wide = piece.astype(F32)
            square += wide * wide
            pieces.append(piece * GA[xx, yy][0:1])
        lhs = jnp.concatenate(pieces, axis=1)
        return jnp.dot(lhs, wgu_v[xx], preferred_element_type=F32), square

    def up(k):
        total, square = part(k, x)
        gather_rest(G.at[k], k, "sides")
        for xx in (right, left):
            more, sq = part(k, xx)
            total, square = total + more, square + sq
        gather_rest(G.at[k], k, "across")
        more, sq = part(k, across)
        total, square = total + more, square + sq
        scale = lax.rsqrt(jnp.sum(square, axis=1, keepdims=True) / plan.d + EPS)
        total = total * scale
        gated = jnp.minimum(total[:, :W], 7.0)
        upper = jnp.clip(total[:, W:], -7.0, 7.0)
        return ((upper + 1.0) * gated * jax.nn.sigmoid(1.702 * gated)).astype(BF16)

    def down(k, hidden):
        for yy in range(ny):
            part_out = jnp.dot(
                hidden, wd_v[:, yy * nx * W : (yy + 1) * nx * W], preferred_element_type=F32
            ).astype(BF16)
            for xx in range(nx):
                PB[k, xx, yy] = part_out[:, xx * W : (xx + 1) * W]

    def sum_send(k):
        for at, dy in enumerate(plan.far):
            way = at % 2
            target, other = (right, left) if way == 0 else (left, right)
            remote(PB.at[k, across, at_y(dy)], XR.at[k, dy], s_xr.at[k, dy], r_xr.at[k, dy], id_x(target))
        for at, dy in enumerate(plan.far):
            way = at % 2
            other = left if way == 0 else right
            remote(
                PB.at[k, other, at_y(dy)],
                XM.at[k, 1 - way, dy],
                s_xm.at[k, 1 - way, dy],
                r_xm.at[k, 1 - way, dy],
                id_x(other),
            )

    def sum_relay(k):
        for at, dy in enumerate(plan.far):
            way = at % 2
            target = right if way == 0 else left
            arrive(XR.at[k, dy], r_xr.at[k, dy])
            both = XR[k, dy].astype(F32) + PB[k, target, at_y(dy)].astype(F32)
            SM[k, dy] = both.astype(BF16)
            remote(
                SM.at[k, dy],
                XM.at[k, way, dy],
                s_xm.at[k, way, dy],
                r_xm.at[k, way, dy],
                id_x(target),
            )

    def sum_y(k):
        for dy in plan.far:
            arrive(XM.at[k, 0, dy], r_xm.at[k, 0, dy])
            arrive(XM.at[k, 1, dy], r_xm.at[k, 1, dy])
            total = (
                PB[k, x, at_y(dy)].astype(F32)
                + XM[k, 0, dy].astype(F32)
                + XM[k, 1, dy].astype(F32)
            )
            if dy == 0:
                return total
            Q[k, dy] = total.astype(BF16)
            remote(
                Q.at[k, dy],
                YL.at[k, (-dy) % ny],
                s_yl.at[k, dy],
                r_yl.at[k, (-dy) % ny],
                id_y(dy),
            )

    def sum_end(k, total):
        for dy in plan.near[1:]:
            arrive(YL.at[k, dy], r_yl.at[k, dy])
            total += YL[k, dy].astype(F32)
        groups = rows // CAP
        RB[k * groups : (k + 1) * groups] = total.reshape(groups, CAP, W).astype(BF16)
        for j in plan.chunks[k][::-1]:
            base = plan.pos[j] * 2
            if j == 0:
                RI[ep] = RB[base + c]
            for core in (0, 1) if j else (1 - c,):
                target = at_z(j) * 2 + core
                index = base + (core if j else 0)
                remote(RB.at[base + core], RI.at[ep], s_ret.at[index], r_ret.at[ep], (target, tp))

    gather_y(GA, 2)
    chunk_in(0)
    gather_y(G.at[0], 0)
    gather_x(GA, 2)
    gather_x(G.at[0], 0)
    gather_relay(GA, 2)
    chunk_in(1)
    gather_y(G.at[1], 1)
    gather_relay(G.at[0], 0)
    gather_x(G.at[1], 1)
    gather_rest(GA, 2, "sides")
    gather_rest(GA, 2, "across")
    for copy in weights:
        copy.wait()
    hidden = up(0)
    gather_relay(G.at[1], 1)
    down(0, hidden)
    sum_send(0)
    hidden = up(1)
    down(1, hidden)
    sum_send(1)
    sum_relay(0)
    sum_relay(1)
    first = sum_y(0)
    second = sum_y(1)
    sum_end(1, second)
    sum_end(0, first)

    for j in range(nz):
        for core in (0, 1) if j else (1 - c,):
            expert = at_z(j) * 2 + core
            arrive(RI.at[expert], r_ret.at[expert])
    returned = RI[...].reshape(lanes, W).astype(F32)
    out[...] = jnp.dot(
        combine, returned, preferred_element_type=F32, precision=lax.Precision.HIGHEST
    ).astype(BF16)
    for copy in pending:
        copy.wait_send()


def run(plan, tokens, norm_gain, routes, route_weights, w_gate, w_up, w_down):
    nz, ny, nx, rows = plan.nz, plan.ny, plan.nx, plan.rows
    groups = 2 * nz
    vmem = pl.BlockSpec(memory_space=pltpu.VMEM)
    hbm = pl.BlockSpec(memory_space=pl.ANY)
    dma = pltpu.SemaphoreType.DMA
    return pl.pallas_call(
        functools.partial(kernel, plan),
        out_shape=jax.ShapeDtypeStruct(tokens.shape, BF16),
        in_specs=[vmem] * 4 + [hbm] * 3,
        out_specs=vmem,
        scratch_shapes=[
            pltpu.VMEM((nx, ny * W, 2 * W), BF16),
            pltpu.VMEM((W, plan.d), BF16),
            pltpu.VMEM((groups, CAP, W), BF16),
            pltpu.VMEM((groups, CAP, W), BF16),
            pltpu.VMEM((2, nx, ny, rows, W), BF16),
            pltpu.VMEM((nx, ny, 8, W), BF16),
            pltpu.VMEM((2, nx, ny, rows, W), BF16),
            pltpu.VMEM((2, ny, rows, W), BF16),
            pltpu.VMEM((2, 2, ny, rows, W), BF16),
            pltpu.VMEM((2, ny, rows, W), BF16),
            pltpu.VMEM((2, ny, rows, W), BF16),
            pltpu.VMEM((2, ny, rows, W), BF16),
            pltpu.VMEM((groups, CAP, W), BF16),
            pltpu.VMEM((groups, CAP, W), BF16),
            dma((3, ny * nx)),
            dma((groups,)),
            dma((groups,)),
            dma((3, ny)),
            dma((3, ny)),
            dma((3, 2, ny)),
            dma((3, 2, ny)),
            dma((3, ny)),
            dma((3, ny)),
            dma((2, ny)),
            dma((2, ny)),
            dma((2, 2, ny)),
            dma((2, 2, ny)),
            dma((2, ny)),
            dma((2, ny)),
            dma((groups,)),
            dma((groups,)),
        ],
        compiler_params=pltpu.CompilerParams(collective_id=0, has_side_effects=True),
        name="moe",
    )(
        tokens,
        norm_gain.reshape(1, W),
        routes,
        route_weights,
        w_gate.reshape(ny * nx, W, W),
        w_up.reshape(ny * nx, W, W),
        w_down.reshape(W, plan.d),
    )


def build(mesh, nz, ny, nx):
    placed = (
        P("ep", "tp"),
        P("tp"),
        P("ep", None),
        P("ep", None),
        P("ep", None, "tp"),
        P("ep", None, "tp"),
        P("ep", "tp", None),
    )
    return jax.shard_map(
        functools.partial(run, Plan(nz, ny, nx)),
        mesh=mesh,
        in_specs=placed,
        out_specs=P("ep", "tp"),
        check_vma=False,
    )


def solution(mesh):
    nx = 4
    return build(mesh, mesh.shape["ep"] // 2, mesh.shape["tp"] // nx, nx)
```

time: 140 us -> 77.6 us (0.55)
  blocking collectives: 93.4 us -> 0 us
  Pallas kernels: 0 us -> 74 us
  waiting for transfers between devices: 18.1 us -> 0 us
  starting transfers between devices: 17.7 us -> 0 us
  matrix products: 4.23 us -> 0 us
  other arithmetic: 3.39 us -> 0 us
    all_to_all x3 -> x0, blocking collectives: 93.4 us -> none  [the longest x1 32.7 us: shards(): lax.all_to_all(outbound.reshape(groups, capacity, -1), 'ep', split_axis=0...]
    pallas_call x0 -> x1, Pallas kernels: none -> 74 us  [run(): pl.pallas_call(functools.partial(kernel, plan), out_shape=jax.ShapeDtypeS...]
    all_to_all x2 -> x0, waiting for transfers between devices: 18.1 us -> none  [the longest x1 12.2 us: shards(): lax.all_to_all(summed.reshape(groups, capacity, -1), 'ep', split_axis=0,...]
    all_to_all x2 -> x0, starting transfers between devices: 17.7 us -> none  [the longest x1 10.5 us: from_everyone(): return lax.all_to_all(copies, axis, split_axis=0, concat_axis=0, tiled=True)]
    dot_general x4 -> x0, matrix products: 4.23 us -> none  [the longest x1 2.08 us: shards(): jnp.dot(hidden, w_down[0], preferred_element_type=jnp.float32)]
    unnamed x7, local copies, waits for them, and re-layouts: 0.77 us -> 3.31 us
    reduce_sum x5 -> x0, other arithmetic: 1.95 us -> none  [the longest x1 0.89 us: shards(): total_sq = of_everyone(jnp.sum(values * values, axis=1), 'tp')]
  transfers between devices with their start and end apart: 2 -> 0, of which waited for: 2 -> 0; matrix products, arithmetic and copies ran while one was open for 2% -> 0% of each run, Pallas kernels for 0% -> 0%
where the time goes in v1:
time: 77.6 us; the launch traced here: 77.3 us
  Pallas kernels  74 us (95%)
  local copies, waits for them, and re-layouts  3.31 us (4%)
    pallas_call x1, Pallas kernels, run(): pl.pallas_call(functools.partial(kernel, plan), out_shape=jax.ShapeDtypeS...  74 us
    unnamed x7, local copies, waits for them, and re-layouts  3.31 us

profile of v1, /device:TPU:1, one launch (start us, length us, event | category | flops | bytes accessed | tf_op | source)
XLA Modules:
  0.0 77.3 jit_solution(13713223043843549716)
XLA Ops:
  0.0 0.0 copy-start
  0.0 0.7 copy-done
  0.7 0.0 copy-start.1
  0.7 0.7 copy.8.routes
  1.4 0.0 copy-done.1
  1.4 0.7 copy.9.rw
  2.0 74.0 %moe.1 = bf16[16,128]{1,0:T(8,128)(2,1)} custom-call(bf16[16,128]{1,0:T(8,128)(2,1)} %tok.1, bf16[1,128]{1,0:T(2,128)(2,1)} %bitcast.7, s32[16,4]{1,0:T(8,128)} %copy.8.routes, f32[16,4]{1,0:T(8,128)} %copy.9.rw, bf16[32,128,128]{2,1,0:T(8,128)(2,1)} %bitcast.4, bf16[32,128,128]{2,1,0:T(8,128)(2,1)} %bitcast.5, bf16[128,4096]{1,0:T(8,128)(2,1)} %bitcast.6), custom_call_target="tpu_custom_call" | custom-call | tf_op jit(solution)/shard_map/moe/pallas_call | solution.py:374
  76.0 1.3 %copy.11 = bf16[16,128]{1,0:T(8,128)(2,1)} copy(bf16[16,128]{1,0:T(8,128)(2,1)} %moe.1) | data formatting | bytes 8192
Async XLA Ops:
  0.0 0.7 copy-start
  0.7 0.7 copy-start.1

commit v2 on v1

v2 whole, which is shorter than its diff:
```python
import functools

import jax
import jax.numpy as jnp
from jax import lax
from jax.experimental import pallas as pl
from jax.experimental.pallas import tpu as pltpu
from jax.sharding import PartitionSpec as P

MESH = pl.DeviceIdType.MESH
BF16 = jnp.bfloat16
F32 = jnp.float32
W = 128
CAP = 4
EPS = 1e-05


def by_distance(n):
    return sorted(range(n), key=lambda j: (min(j, n - j), j))


class Plan:
    def __init__(self, nz, ny, nx):
        self.nz, self.ny, self.nx = nz, ny, nx
        self.experts = 2 * nz
        self.tp = ny * nx
        self.d = self.tp * W
        ring = by_distance(nz)
        self.chunks = [ring[nz // 2 :], ring[: nz // 2]]
        self.pos = {j: at for at, j in enumerate(self.chunks[0] + self.chunks[1])}
        self.rows = (nz // 2) * 2 * CAP
        self.near = by_distance(ny)
        self.far = self.near[::-1]


def kernel(
    plan,
    tok,
    gain,
    routes,
    rw,
    wg,
    wu,
    wd,
    out,
    wgu_v,
    wd_v,
    ob,
    lb,
    G,
    GA,
    PB,
    XM,
    Q,
    YL,
    RB,
    RI,
    lb2,
    YL2,
    RB2,
    RI2,
    both,
    tok_v,
    gain_v,
    routes_v,
    rw_v,
    s_in,
    s_w,
    s_z,
    s_p,
    r_z,
    r_ga,
    r_gy,
    r_gx,
    r_xm,
    r_yl,
):
    nz, ny, nx, rows = plan.nz, plan.ny, plan.nx, plan.rows
    ep = lax.axis_index("ep")
    tp = lax.axis_index("tp")
    z, c = ep // 2, ep % 2
    y, x = tp // nx, tp % nx

    def at_z(j):
        return (z + j) % nz

    def at_y(dy):
        return (y + dy) % ny

    def id_z(j, core):
        return (at_z(j) * 2 + core, tp)

    def id_y(dy):
        return (ep, at_y(dy) * nx + x)

    def at_x(dx):
        return (x + dx) % nx

    def id_x(dx):
        return (ep, y * nx + at_x(dx))

    sides = [2, 1, 3]
    sides_of = (sides, [1, 3])
    half = [j for j in range(nz) if j in plan.chunks[1] or (-j) % nz in plan.chunks[1]]
    peers = [id_z(j, core) for j in range(1, nz) for core in (0, 1)]
    peers += [id_z(0, 1 - c)]
    peers += [id_y(dy) for dy in range(1, ny)]
    peers += [id_x(dx) for dx in sides]
    facing = y * nx + at_x(2)
    peers += [
        (at_z(j) * 2 + core, facing) for j in half for core in ((0, 1) if j else (1 - c,))
    ]
    barrier = pltpu.get_barrier_semaphore()
    for peer in peers:
        pl.semaphore_signal(barrier, inc=1, device_id=peer, device_id_type=MESH)

    small = [
        pltpu.make_async_copy(src, dst, s_in.at[at])
        for at, (src, dst) in enumerate(
            ((routes, routes_v), (tok, tok_v), (rw, rw_v), (gain, gain_v))
        )
    ]
    for copy in small:
        copy.start()
    for yy in range(ny):
        for xx in range(nx):
            for half, src in enumerate((wg, wu)):
                pltpu.make_async_copy(
                    src.at[yy * nx + xx],
                    wgu_v.at[xx, pl.ds(yy * W, W), pl.ds(half * W, W)],
                    s_w.at[0],
                ).start()
    pltpu.make_async_copy(wd, wd_v, s_w.at[1]).start()
    for copy in small:
        copy.wait()

    tokens = tok.shape[0]
    slots = plan.experts * CAP
    slot_id = lax.broadcasted_iota(jnp.int32, (slots, tokens), 0)
    expert_of = slot_id // CAP
    named = jnp.zeros((slots, tokens), F32)
    weight = jnp.zeros((slots, tokens), F32)
    for k in range(routes.shape[0]):
        same = routes_v[k : k + 1, :] == expert_of
        named = jnp.where(same, 1.0, named)
        weight = jnp.where(same, rw_v[k : k + 1, :], weight)
    before = (
        lax.broadcasted_iota(jnp.int32, (tokens, tokens), 0)
        < lax.broadcasted_iota(jnp.int32, (tokens, tokens), 1)
    ).astype(F32)
    earlier = jnp.dot(named, before, preferred_element_type=F32)
    pick = jnp.where(earlier == (slot_id % CAP).astype(F32), named, 0.0)
    combine = weight * pick
    outbound = jnp.dot(pick.astype(BF16), tok_v[...], preferred_element_type=F32)
    ob[...] = outbound.reshape(plan.experts, CAP, W).astype(BF16)
    GA[x, y] = jnp.broadcast_to(gain_v[...], (8, W))
    lb[2 * plan.pos[0] + c] = ob[ep]

    def remote(src, dst, send, recv, device):
        pltpu.make_async_remote_copy(
            src_ref=src,
            dst_ref=dst,
            send_sem=send,
            recv_sem=recv,
            device_id=device,
            device_id_type=MESH,
        ).start()

    def arrive(ref, sem):
        pltpu.make_async_copy(ref, ref, sem).wait()

    pl.semaphore_wait(barrier, len(peers))

    for j in by_distance(nz)[::-1]:
        landing = plan.pos[(-j) % nz] * 2 + c
        k = 0 if (-j) % nz in plan.chunks[0] else 1
        for core in (0, 1) if j else (1 - c,):
            target = at_z(j) * 2 + core
            remote(ob.at[target], lb.at[landing], s_z.at[0], r_z.at[k], (target, tp))

    groups = rows // CAP
    for j in by_distance(nz)[::-1]:
        back = (-j) % nz
        if back in plan.chunks[1]:
            landing = plan.pos[back] * 2 - groups + c
            for core in (0, 1):
                target = at_z(j) * 2 + core
                remote(ob.at[target], lb2.at[landing], s_z.at[2], r_z.at[3], (target, facing))

    def chunk_in(k):
        arrive(lb.at[pl.ds(0, groups - (1 if k else 0))], r_z.at[k])
        G[k, x, y] = lb[k * groups : (k + 1) * groups].reshape(rows, W)

    def facing_in():
        arrive(lb2, r_z.at[3])
        G[1, at_x(2), y] = lb2[...].reshape(rows, W)
        for dy in plan.far[:-1]:
            here = G.at[1, at_x(2), y]
            remote(here, here, s_p.at[5, 0], r_gx.at[1, 2], id_y(dy))

    def gain_y():
        for dy in plan.far[:-1]:
            remote(GA.at[x, y], GA.at[x, y], s_p.at[4, 0], r_ga.at[0], id_y(dy))

    def gain_x():
        arrive(GA.at[0, pl.ds(0, ny - 1)], r_ga.at[0])
        for dx in sides:
            remote(GA.at[x], GA.at[x], s_p.at[4, 1], r_ga.at[1], id_x(dx))

    def gain_in():
        arrive(GA.at[pl.ds(0, nx - 1)], r_ga.at[1])

    def gather_y(k):
        for dy in plan.far[:-1]:
            here = G.at[k, x, y]
            remote(here, here, s_p.at[k, 0], r_gy.at[k, (-dy) % ny], id_y(dy))

    def gather_x(k, at):
        dy = plan.near[at]
        here = G.at[k, x, at_y(dy)]
        if dy:
            arrive(here, r_gy.at[k, dy])
        for dx in sides_of[k]:
            remote(here, here, s_p.at[k, 1], r_gx.at[k, (-dx) % nx], id_x(dx))

    def part(k, xx):
        pieces, square = [], jnp.zeros((rows, W), F32)
        for yy in range(ny):
            piece = G[k, xx, yy]
            wide = piece.astype(F32)
            square += wide * wide
            pieces.append(piece * GA[xx, yy][0:1])
        lhs = jnp.concatenate(pieces, axis=1)
        return jnp.dot(lhs, wgu_v[xx], preferred_element_type=F32), square

    def up(k):
        total, square = part(k, x)
        for dx in sides[::-1]:
            if k == 1 and dx == 2:
                arrive(G.at[k, at_x(dx), pl.ds(0, ny - 1)], r_gx.at[k, dx])
            else:
                arrive(G.at[k, at_x(dx)], r_gx.at[k, dx])
            more, sq = part(k, at_x(dx))
            total, square = total + more, square + sq
        scale = lax.rsqrt(jnp.sum(square, axis=1, keepdims=True) / plan.d + EPS)
        total = total * scale
        gated = jnp.minimum(total[:, :W], 7.0)
        upper = jnp.clip(total[:, W:], -7.0, 7.0)
        return ((upper + 1.0) * gated * jax.nn.sigmoid(1.702 * gated)).astype(BF16)

    def down(k, hidden):
        for yy in range(ny):
            part_out = jnp.dot(
                hidden, wd_v[:, yy * nx * W : (yy + 1) * nx * W], preferred_element_type=F32
            ).astype(BF16)
            for xx in range(nx):
                PB[k, xx, yy] = part_out[:, xx * W : (xx + 1) * W]

    def sum_x(k):
        for dy in plan.far:
            for dx in sides_of[k]:
                remote(
                    PB.at[k, at_x(dx), at_y(dy)],
                    XM.at[k, dy, (-dx) % nx - 1],
                    s_p.at[2 + k, 1],
                    r_xm.at[k, dy],
                    id_x(dx),
                )

    def facing_out():
        for dy in plan.far[:-1]:
            slot = (-dy) % ny - 1
            remote(PB.at[1, at_x(2), at_y(dy)], YL2.at[slot], s_p.at[5, 1], r_yl.at[2], id_y(dy))

    def sum_y(k):
        for dy in plan.far:
            arrive(XM.at[k, dy, pl.ds(0, len(sides_of[k]))], r_xm.at[k, dy])
            total = PB[k, x, at_y(dy)].astype(F32)
            for dx in sides_of[k]:
                total += XM[k, dy, dx - 1].astype(F32)
            if dy:
                Q[k, dy] = total.astype(BF16)
                slot = (-dy) % ny - 1
                remote(Q.at[k, dy], YL.at[k, slot], s_p.at[2 + k, 0], r_yl.at[k], id_y(dy))
        return total

    def sum_end(k, total):
        arrive(YL.at[k], r_yl.at[k])
        for dy in range(1, ny):
            total += YL[k, dy - 1].astype(F32)
        RB[k * groups : (k + 1) * groups] = total.reshape(groups, CAP, W).astype(BF16)

    def facing_end():
        total = PB[1, at_x(2), y].astype(F32)
        arrive(YL2, r_yl.at[2])
        for dy in range(1, ny):
            total += YL2[dy - 1].astype(F32)
        RB2[...] = total.reshape(groups, CAP, W).astype(BF16)
        for j in plan.chunks[1][::-1]:
            base = 2 * plan.pos[j] - groups
            for core in (0, 1):
                remote(
                    RB2.at[base + core],
                    RI2.at[base + c],
                    s_z.at[3],
                    r_z.at[4],
                    (at_z(j) * 2 + core, facing),
                )

    def give_back(k):
        for j in plan.chunks[k][::-1]:
            base = 2 * plan.pos[j]
            if j == 0:
                RI[ep] = RB[base + c]
            for core in (0, 1) if j else (1 - c,):
                remote(RB.at[base + core], RI.at[ep], s_z.at[1], r_z.at[2], id_z(j, core))

    gain_y()
    chunk_in(1)
    gather_y(1)
    gather_x(1, 0)
    chunk_in(0)
    gather_y(0)
    gather_x(0, 0)
    facing_in()
    gain_x()
    for at in range(1, ny):
        gather_x(1, at)
    for at in range(1, ny):
        gather_x(0, at)
    gain_in()
    arrive(wgu_v, s_w.at[0])
    hidden = up(0)
    arrive(wd_v, s_w.at[1])
    down(0, hidden)
    sum_x(0)
    hidden = up(1)
    down(1, hidden)
    sum_x(1)
    facing_out()
    far = sum_y(0)
    near = sum_y(1)
    sum_end(0, far)
    give_back(0)
    facing_end()
    sum_end(1, near)
    give_back(1)
    arrive(RI2, r_z.at[4])
    arrive(RI.at[pl.ds(0, plan.experts - 1)], r_z.at[2])
    both[...] = RI[...].astype(F32)
    for j in plan.chunks[1]:
        base = 2 * plan.pos[j] - groups
        for core in (0, 1):
            expert = at_z(-j) * 2 + core
            both[expert] = both[expert] + RI2[base + core].astype(F32)
    returned = both[...].reshape(slots, W)
    out[...] = lax.dot_general(
        combine,
        returned,
        (((0,), (0,)), ((), ())),
        preferred_element_type=F32,
        precision=lax.Precision.HIGHEST,
    ).astype(BF16)

    for at in range(2):
        arrive(lb.at[pl.ds(0, plan.experts - 1)], s_z.at[at])
    for k in range(2):
        for buf, at in ((G, k), (PB, 2 + k)):
            arrive(buf.at[k, 0, pl.ds(0, ny - 1)], s_p.at[at, 0])
            arrive(buf.at[k, pl.ds(0, len(sides_of[k]))], s_p.at[at, 1])
    for at in range(2):
        arrive(lb2, s_z.at[2 + at])
        arrive(G.at[1, 0, pl.ds(0, ny - 1)], s_p.at[5, at])
    arrive(GA.at[0, pl.ds(0, ny - 1)], s_p.at[4, 0])
    arrive(GA.at[pl.ds(0, nx - 1)], s_p.at[4, 1])


def run(plan, tokens, norm_gain, routes, route_weights, w_gate, w_up, w_down):
    nz, ny, nx, rows = plan.nz, plan.ny, plan.nx, plan.rows
    groups = 2 * nz
    vmem = pl.BlockSpec(memory_space=pltpu.VMEM)
    hbm = pl.BlockSpec(memory_space=pl.ANY)
    dma = pltpu.SemaphoreType.DMA
    return pl.pallas_call(
        functools.partial(kernel, plan),
        out_shape=jax.ShapeDtypeStruct(tokens.shape, BF16),
        in_specs=[hbm] * 7,
        out_specs=vmem,
        scratch_shapes=[
            pltpu.VMEM((nx, ny * W, 2 * W), BF16),
            pltpu.VMEM((W, plan.d), BF16),
            pltpu.VMEM((groups, CAP, W), BF16),
            pltpu.VMEM((groups, CAP, W), BF16),
            pltpu.VMEM((2, nx, ny, rows, W), BF16),
            pltpu.VMEM((nx, ny, 8, W), BF16),
            pltpu.VMEM((2, nx, ny, rows, W), BF16),
            pltpu.VMEM((2, ny, nx - 1, rows, W), BF16),
            pltpu.VMEM((2, ny, rows, W), BF16),
            pltpu.VMEM((2, ny - 1, rows, W), BF16),
            pltpu.VMEM((groups, CAP, W), BF16),
            pltpu.VMEM((groups, CAP, W), BF16),
            pltpu.VMEM((rows // CAP, CAP, W), BF16),
            pltpu.VMEM((ny - 1, rows, W), BF16),
            pltpu.VMEM((rows // CAP, CAP, W), BF16),
            pltpu.VMEM((rows // CAP, CAP, W), BF16),
            pltpu.VMEM((groups, CAP, W), F32),
            pltpu.VMEM(tokens.shape, BF16),
            pltpu.VMEM((1, W), BF16),
            pltpu.VMEM(routes.shape[::-1], jnp.int32),
            pltpu.VMEM(routes.shape[::-1], F32),
            dma((4,)),
            dma((2,)),
            dma((4,)),
            dma((6, 2)),
            dma((5,)),
            dma((2,)),
            dma((2, ny)),
            dma((2, nx)),
            dma((2, ny)),
            dma((3,)),
        ],
        compiler_params=pltpu.CompilerParams(collective_id=0, has_side_effects=True),
        name="moe",
    )(
        tokens,
        norm_gain.reshape(1, W),
        routes.T,
        route_weights.T,
        w_gate.reshape(ny * nx, W, W),
        w_up.reshape(ny * nx, W, W),
        w_down.reshape(W, plan.d),
    )


def build(mesh, nz, ny, nx):
    placed = (
        P("ep", "tp"),
        P("tp"),
        P("ep", None),
        P("ep", None),
        P("ep", None, "tp"),
        P("ep", None, "tp"),
        P("ep", "tp", None),
    )
    return jax.shard_map(
        functools.partial(run, Plan(nz, ny, nx)),
        mesh=mesh,
        in_specs=placed,
        out_specs=P("ep", "tp"),
        check_vma=False,
    )


def solution(mesh):
    nx = 4
    return build(mesh, mesh.shape["ep"] // 2, mesh.shape["tp"] // nx, nx)
```

time: 77.6 us -> 66.9 us (0.86)
  Pallas kernels: 74 us -> 65.4 us
  local copies, waits for them, and re-layouts: 3.31 us -> 1.28 us
    pallas_call x1, Pallas kernels: 74 us -> 65.4 us  [run(): pl.pallas_call(functools.partial(kernel, plan), out_shape=jax.ShapeDtypeS...]
    unnamed x7 -> x1, local copies, waits for them, and re-layouts: 3.31 us -> 1.28 us
where the time goes in v2:
time: 66.9 us; the launch traced here: 66.7 us
  Pallas kernels  65.4 us (98%)
  local copies, waits for them, and re-layouts  1.28 us (2%)
    pallas_call x1, Pallas kernels, run(): pl.pallas_call(functools.partial(kernel, plan), out_shape=jax.ShapeDtypeS...  65.4 us

profile of v2, /device:TPU:1, one launch (start us, length us, event | category | flops | bytes accessed | tf_op | source)
XLA Modules:
  0.0 66.7 jit_solution(7204062049203963368)
XLA Ops:
  0.0 65.4 %moe.1 = bf16[16,128]{1,0:T(8,128)(2,1)} custom-call(bf16[16,128]{1,0:T(8,128)(2,1)} %tok.1, bf16[1,128]{1,0:T(2,128)(2,1)} %bitcast.11, s32[4,16]{1,0:T(4,128)} %bitcast.9, f32[4,16]{1,0:T(4,128)} %bitcast.10, bf16[32,128,128]{2,1,0:T(8,128)(2,1)} %bitcast.6, bf16[32,128,128]{2,1,0:T(8,128)(2,1)} %bitcast.7, bf16[128,4096]{1,0:T(8,128)(2,1)} %bitcast.8), custom_call_target="tpu_custom_call" | custom-call | tf_op jit(solution)/shard_map/moe/pallas_call | solution.py:384
  65.4 1.3 %copy.9 = bf16[16,128]{1,0:T(8,128)(2,1)} copy(bf16[16,128]{1,0:T(8,128)(2,1)} %moe.1) | data formatting | bytes 8192

commit v3 on v2

--- a/solution.py
+++ b/solution.py
@@ -59,7 +59,6 @@
     YL2,
     RB2,
     RI2,
-    both,
     tok_v,
     gain_v,
     routes_v,
@@ -248,35 +247,38 @@
         upper = jnp.clip(total[:, W:], -7.0, 7.0)
         return ((upper + 1.0) * gated * jax.nn.sigmoid(1.702 * gated)).astype(BF16)
 
-    def down(k, hidden):
-        for yy in range(ny):
-            part_out = jnp.dot(
-                hidden, wd_v[:, yy * nx * W : (yy + 1) * nx * W], preferred_element_type=F32
-            ).astype(BF16)
+    def down(k, hidden, send):
+        for dy in plan.far:
+            yy = at_y(dy)
+            columns = pl.ds(pl.multiple_of(yy * (nx * W), nx * W), nx * W)
+            part_out = jnp.dot(hidden, wd_v[:, columns], preferred_element_type=F32).astype(BF16)
             for xx in range(nx):
                 PB[k, xx, yy] = part_out[:, xx * W : (xx + 1) * W]
-
-    def sum_x(k):
-        for dy in plan.far:
-            for dx in sides_of[k]:
-                remote(
-                    PB.at[k, at_x(dx), at_y(dy)],
-                    XM.at[k, dy, (-dx) % nx - 1],
-                    s_p.at[2 + k, 1],
-                    r_xm.at[k, dy],
-                    id_x(dx),
-                )
-
-    def facing_out():
+            if send:
+                sum_x(k, dy)
+
+    def sum_x(k, dy):
+        for dx in (1, 3):
+            remote(
+                PB.at[k, at_x(dx), at_y(dy)],
+                XM.at[k, dy, (-dx) % nx - 1],
+                s_p.at[2 + k, 1],
+                r_xm.at[k, dy],
+                id_x(dx),
+            )
+
+    def facing_out(k):
         for dy in plan.far[:-1]:
             slot = (-dy) % ny - 1
-            remote(PB.at[1, at_x(2), at_y(dy)], YL2.at[slot], s_p.at[5, 1], r_yl.at[2], id_y(dy))
+            remote(
+                PB.at[k, at_x(2), at_y(dy)], YL2.at[k, slot], s_p.at[6, k], r_yl.at[2 + k], id_y(dy)
+            )
 
     def sum_y(k):
         for dy in plan.far:
-            arrive(XM.at[k, dy, pl.ds(0, len(sides_of[k]))], r_xm.at[k, dy])
+            arrive(XM.at[k, dy, pl.ds(0, 2)], r_xm.at[k, dy])
             total = PB[k, x, at_y(dy)].astype(F32)
-            for dx in sides_of[k]:
+            for dx in (1, 3):
                 total += XM[k, dy, dx - 1].astype(F32)
             if dy:
                 Q[k, dy] = total.astype(BF16)
@@ -290,18 +292,18 @@
             total += YL[k, dy - 1].astype(F32)
         RB[k * groups : (k + 1) * groups] = total.reshape(groups, CAP, W).astype(BF16)
 
-    def facing_end():
-        total = PB[1, at_x(2), y].astype(F32)
-        arrive(YL2, r_yl.at[2])
+    def facing_end(k):
+        total = PB[k, at_x(2), y].astype(F32)
+        arrive(YL2.at[k], r_yl.at[2 + k])
         for dy in range(1, ny):
-            total += YL2[dy - 1].astype(F32)
-        RB2[...] = total.reshape(groups, CAP, W).astype(BF16)
-        for j in plan.chunks[1][::-1]:
-            base = 2 * plan.pos[j] - groups
+            total += YL2[k, dy - 1].astype(F32)
+        RB2[k * groups : (k + 1) * groups] = total.reshape(groups, CAP, W).astype(BF16)
+        for j in plan.chunks[k][::-1]:
+            base = 2 * plan.pos[j]
             for core in (0, 1):
                 remote(
                     RB2.at[base + core],
-                    RI2.at[base + c],
+                    RI2.at[ep],
                     s_z.at[3],
                     r_z.at[4],
                     (at_z(j) * 2 + core, facing),
@@ -330,47 +332,44 @@
         gather_x(0, at)
     gain_in()
     arrive(wgu_v, s_w.at[0])
-    hidden = up(0)
     arrive(wd_v, s_w.at[1])
-    down(0, hidden)
-    sum_x(0)
-    hidden = up(1)
-    down(1, hidden)
-    sum_x(1)
-    facing_out()
+    down(1, up(1), False)
+    facing_out(1)
+    down(0, up(0), True)
+    facing_out(0)
+    for dy in plan.far:
+        sum_x(1, dy)
     far = sum_y(0)
     near = sum_y(1)
+    facing_end(0)
+    facing_end(1)
     sum_end(0, far)
     give_back(0)
-    facing_end()
     sum_end(1, near)
     give_back(1)
     arrive(RI2, r_z.at[4])
     arrive(RI.at[pl.ds(0, plan.experts - 1)], r_z.at[2])
-    both[...] = RI[...].astype(F32)
-    for j in plan.chunks[1]:
-        base = 2 * plan.pos[j] - groups
-        for core in (0, 1):
-            expert = at_z(-j) * 2 + core
-            both[expert] = both[expert] + RI2[base + core].astype(F32)
-    returned = both[...].reshape(slots, W)
+    returned = (RI[...].astype(F32) + RI2[...].astype(F32)).reshape(slots, W)
     out[...] = lax.dot_general(
         combine,
         returned,
         (((0,), (0,)), ((), ())),
         preferred_element_type=F32,
         precision=lax.Precision.HIGHEST,
-    ).astype(BF16)
+    )
 
     for at in range(2):
         arrive(lb.at[pl.ds(0, plan.experts - 1)], s_z.at[at])
+    arrive(lb2, s_z.at[2])
+    arrive(lb, s_z.at[3])
     for k in range(2):
-        for buf, at in ((G, k), (PB, 2 + k)):
-            arrive(buf.at[k, 0, pl.ds(0, ny - 1)], s_p.at[at, 0])
-            arrive(buf.at[k, pl.ds(0, len(sides_of[k]))], s_p.at[at, 1])
-    for at in range(2):
-        arrive(lb2, s_z.at[2 + at])
-        arrive(G.at[1, 0, pl.ds(0, ny - 1)], s_p.at[5, at])
+        row = pl.ds(0, ny - 1)
+        arrive(G.at[k, 0, row], s_p.at[k, 0])
+        arrive(G.at[k, pl.ds(0, len(sides_of[k]))], s_p.at[k, 1])
+        arrive(PB.at[k, 0, row], s_p.at[2 + k, 0])
+        arrive(PB.at[k, pl.ds(0, 2)], s_p.at[2 + k, 1])
+        arrive(PB.at[k, 0, row], s_p.at[6, k])
+    arrive(G.at[1, 0, pl.ds(0, ny - 1)], s_p.at[5, 0])
     arrive(GA.at[0, pl.ds(0, ny - 1)], s_p.at[4, 0])
     arrive(GA.at[pl.ds(0, nx - 1)], s_p.at[4, 1])
 
@@ -383,7 +382,7 @@
     dma = pltpu.SemaphoreType.DMA
     return pl.pallas_call(
         functools.partial(kernel, plan),
-        out_shape=jax.ShapeDtypeStruct(tokens.shape, BF16),
+        out_shape=pltpu.VMEM(tokens.shape, F32),
         in_specs=[hbm] * 7,
         out_specs=vmem,
         scratch_shapes=[
@@ -400,10 +399,9 @@
             pltpu.VMEM((groups, CAP, W), BF16),
             pltpu.VMEM((groups, CAP, W), BF16),
             pltpu.VMEM((rows // CAP, CAP, W), BF16),
-            pltpu.VMEM((ny - 1, rows, W), BF16),
-            pltpu.VMEM((rows // CAP, CAP, W), BF16),
-            pltpu.VMEM((rows // CAP, CAP, W), BF16),
-            pltpu.VMEM((groups, CAP, W), F32),
+            pltpu.VMEM((2, ny - 1, rows, W), BF16),
+            pltpu.VMEM((groups, CAP, W), BF16),
+            pltpu.VMEM((groups, CAP, W), BF16),
             pltpu.VMEM(tokens.shape, BF16),
             pltpu.VMEM((1, W), BF16),
             pltpu.VMEM(routes.shape[::-1], jnp.int32),
@@ -411,13 +409,13 @@
             dma((4,)),
             dma((2,)),
             dma((4,)),
-            dma((6, 2)),
+            dma((7, 2)),
             dma((5,)),
             dma((2,)),
             dma((2, ny)),
             dma((2, nx)),
             dma((2, ny)),
-            dma((3,)),
+            dma((4,)),
         ],
         compiler_params=pltpu.CompilerParams(collective_id=0, has_side_effects=True),
         name="moe",
@@ -429,7 +427,7 @@
         w_gate.reshape(ny * nx, W, W),
         w_up.reshape(ny * nx, W, W),
         w_down.reshape(W, plan.d),
-    )
+    ).astype(BF16)
 
 
 def build(mesh, nz, ny, nx):

time: 66.9 us -> 63.8 us (0.954)
  Pallas kernels: 65.4 us -> 63.1 us
  local copies, waits for them, and re-layouts: 1.28 us -> 0 us
    pallas_call x1, Pallas kernels: 65.4 us -> 63.1 us  [run(): pl.pallas_call(functools.partial(kernel, plan), out_shape=pltpu.VMEM(toke...]
    unnamed x1 -> x0, local copies, waits for them, and re-layouts: 1.28 us -> none
where the time goes in v3:
time: 63.8 us; the launch traced here: 63.7 us
  Pallas kernels  63.1 us (99%)
    pallas_call x1, Pallas kernels, run(): pl.pallas_call(functools.partial(kernel, plan), out_shape=pltpu.VMEM(toke...  63.1 us

profile of v3, /device:TPU:1, one launch (start us, length us, event | category | flops | bytes accessed | tf_op | source)
XLA Modules:
  0.0 63.7 jit_solution(9709916736258710753)
XLA Ops:
  0.0 63.1 %moe.1 = f32[16,128]{1,0:T(8,128)S(1)} custom-call(bf16[16,128]{1,0:T(8,128)(2,1)} %tok.1, bf16[1,128]{1,0:T(2,128)(2,1)} %bitcast.11, s32[4,16]{1,0:T(4,128)} %bitcast.9, f32[4,16]{1,0:T(4,128)} %bitcast.10, bf16[32,128,128]{2,1,0:T(8,128)(2,1)} %bitcast.6, bf16[32,128,128]{2,1,0:T(8,128)(2,1)} %bitcast.7, bf16[128,4096]{1,0:T(8,128)(2,1)} %bitcast.8), custom_call_target="tpu_custom_call" | custom-call | tf_op jit(solution)/shard_map/moe/pallas_call | solution.py:383
  63.1 0.6 convert_element_type.3

commit v4 on v3

--- a/solution.py
+++ b/solution.py
@@ -101,7 +101,7 @@
     sides = [2, 1, 3]
     sides_of = (sides, [1, 3])
     half = [j for j in range(nz) if j in plan.chunks[1] or (-j) % nz in plan.chunks[1]]
-    peers = [id_z(j, core) for j in range(1, nz) for core in (0, 1)]
+    peers = [id_z(j, core) for j in by_distance(nz)[:0:-1] for core in (0, 1)]
     peers += [id_z(0, 1 - c)]
     peers += [id_y(dy) for dy in range(1, ny)]
     peers += [id_x(dx) for dx in sides]
@@ -121,15 +121,6 @@
     ]
     for copy in small:
         copy.start()
-    for yy in range(ny):
-        for xx in range(nx):
-            for half, src in enumerate((wg, wu)):
-                pltpu.make_async_copy(
-                    src.at[yy * nx + xx],
-                    wgu_v.at[xx, pl.ds(yy * W, W), pl.ds(half * W, W)],
-                    s_w.at[0],
-                ).start()
-    pltpu.make_async_copy(wd, wd_v, s_w.at[1]).start()
     for copy in small:
         copy.wait()
 
@@ -318,6 +309,15 @@
                 remote(RB.at[base + core], RI.at[ep], s_z.at[1], r_z.at[2], id_z(j, core))
 
     gain_y()
+    for yy in range(ny):
+        for xx in range(nx):
+            for half, src in enumerate((wg, wu)):
+                pltpu.make_async_copy(
+                    src.at[yy * nx + xx],
+                    wgu_v.at[xx, pl.ds(yy * W, W), pl.ds(half * W, W)],
+                    s_w.at[0],
+                ).start()
+    pltpu.make_async_copy(wd, wd_v, s_w.at[1]).start()
     chunk_in(1)
     gather_y(1)
     gather_x(1, 0)

time: 63.8 us -> 64.1 us (level)
  no operation moved by 1% of the time
where the time goes in v4:
time: 64.1 us; the launch traced here: 64 us
  Pallas kernels  63.4 us (99%)
    pallas_call x1, Pallas kernels, run(): pl.pallas_call(functools.partial(kernel, plan), out_shape=pltpu.VMEM(toke...  63.4 us

profile of v4, /device:TPU:1, one launch (start us, length us, event | category | flops | bytes accessed | tf_op | source)
XLA Modules:
  0.0 64.0 jit_solution(8671386921614908573)
XLA Ops:
  0.0 63.4 %moe.1 = f32[16,128]{1,0:T(8,128)S(1)} custom-call(bf16[16,128]{1,0:T(8,128)(2,1)} %tok.1, bf16[1,128]{1,0:T(2,128)(2,1)} %bitcast.11, s32[4,16]{1,0:T(4,128)} %bitcast.9, f32[4,16]{1,0:T(4,128)} %bitcast.10, bf16[32,128,128]{2,1,0:T(8,128)(2,1)} %bitcast.6, bf16[32,128,128]{2,1,0:T(8,128)(2,1)} %bitcast.7, bf16[128,4096]{1,0:T(8,128)(2,1)} %bitcast.8), custom_call_target="tpu_custom_call" | custom-call | tf_op jit(solution)/shard_map/moe/pallas_call | solution.py:383
  63.4 0.6 convert_element_type.3
